TPU v7x, 32 devices: a whole 2x2x4 slice. The times are simulated.
32 devices in a mesh: sp: 8 (over z, y), tp: 4 (over x, core).
Axes of the slice: x: 2, y: 2, z: 4, core: 2. Of those that a mesh axis runs over, the one named last changes fastest.
Arguments:
- stream: bfloat16 [2048, 2048], P('sp'), may hold values from -3 to 3
- first_group_queries: bfloat16 [2048, 512], P('sp', 'tp'), may hold values from -6 to 6
- first_group_keys: bfloat16 [2048, 512], P('sp', 'tp'), may hold values from -6 to 6
- first_group_values: bfloat16 [2048, 1024], P('sp', 'tp'), may hold values from -5.5 to 5.5
- first_gate_logits: bfloat16 [2048, 1024], P('sp', 'tp'), may hold values from -6 to 6
- first_decay_logits: bfloat16 [2048, 512], P('sp', 'tp'), may hold values from -4.75 to 14.5
- second_group_queries: bfloat16 [2048, 1024], P('sp', 'tp'), may hold values from -6 to 6
- second_group_keys: bfloat16 [2048, 1024], P('sp', 'tp'), may hold values from -6 to 6
- second_group_values: bfloat16 [2048, 1024], P('sp', 'tp'), may hold values from -5.5 to 5.5
- second_gate_logits: bfloat16 [2048, 1024], P('sp', 'tp'), may hold values from -6 to 6
- second_decay_logits: bfloat16 [2048, 1024], P('sp', 'tp'), may hold values from -4.75 to 14.5
- position_log_decay: float32 [2048], P('sp'), may hold values from -0.6932 to 0, as said below
- per_head_norm_gain: float32 [128], replicated, may hold values from 0.1 to 1.9
- first_output_weight: bfloat16 [1024, 2048], P('tp'), may hold values from -0.125 to 0.125
- second_output_weight: bfloat16 [1024, 2048], P('tp'), may hold values from -0.125 to 0.125
- feedforward_norm_gain: float32 [2048], replicated, may hold values from 0.1 to 1.9
- gate_weight: bfloat16 [2048, 5632], P('sp', 'tp'), may hold values from -0.125 to 0.125
- up_weight: bfloat16 [2048, 5632], P('sp', 'tp'), may hold values from -0.125 to 0.125
- down_weight: bfloat16 [5632, 2048], P('tp', 'sp'), may hold values from -0.078125 to 0.078125
Outputs:
- refined: bfloat16 [2048, 2048], P(('sp', 'tp'))
Inputs may be any that keep to these rules, and one draw needn't show every extreme that they name: `position_log_decay`: most positions carry 0.
All inputs are finite; a program needn't handle non-finite values.
Results may differ from a plain program's by a relative error of at most 0.018.
Values may be sent and summed in bfloat16 or wider, within the bound.
A program may use at most 64 MiB of HBM per device.

v0:
```python
import jax
import jax.numpy as jnp
from jax import lax
from jax.sharding import PartitionSpec as P

KEY_SIZE_FIRST = 64
KEY_SIZE_SECOND = 128
DV = 128
BLK = 64
decay_softness = 16.0
norm_eps = 1e-06
highest = lax.Precision.HIGHEST


def channel_log_decays(decay_logits, position_log_decay, key_channels):
    channel_log_decay = (
        jax.nn.log_sigmoid(decay_logits.astype(jnp.float32)) / decay_softness
        + position_log_decay[:, None]
    )
    return channel_log_decay.reshape(decay_logits.shape[0], -1, key_channels)


def one_way(query_matrix, key_matrix, value_matrix, channel_log_decay, start_state):
    length, heads, key_channels = query_matrix.shape
    value_width = value_matrix.shape[-1]
    block_count = length // BLK

    def blocks(member):
        return member.reshape(block_count, BLK, heads, member.shape[-1]).transpose(0, 2, 1, 3)

    query_blocks = blocks(query_matrix)
    key_blocks = blocks(key_matrix)
    value_blocks = blocks(value_matrix)
    running = jnp.cumsum(blocks(channel_log_decay), axis=2)
    block_last = running[:, :, -1:, :]
    query_in = query_blocks * jnp.exp(running)
    key_in = key_blocks * jnp.exp(-running)
    key_end = key_blocks * jnp.exp(block_last - running)
    places = jnp.arange(BLK, dtype=jnp.int32)
    lower = places[:, None] >= places[None, :]
    scores = jnp.where(
        lower, jnp.einsum("nhid,nhjd->nhij", query_in, key_in, precision=highest), 0.0
    )
    local_out = jnp.einsum("nhij,nhjv->nhiv", scores, value_blocks, precision=highest)

    def advance(states, inputs):
        query_part, key_part, value_part, last_part = inputs
        emitted = jnp.einsum("hid,hdv->hiv", query_part, states, precision=highest)
        states = states * jnp.exp(last_part)[:, 0, :, None] + jnp.einsum(
            "hjd,hjv->hdv", key_part, value_part, precision=highest
        )
        return (states, emitted)

    _, carried = lax.scan(advance, start_state, (query_in, key_end, value_blocks, block_last))
    return (local_out + carried).transpose(0, 2, 1, 3).reshape(length, heads, value_width)


def prepare_inputs(
    query_matrix, key_matrix, value_matrix, decay_logits, position_log_decay, key_channels
):
    length = query_matrix.shape[0]
    channel_log_decay = channel_log_decays(decay_logits, position_log_decay, key_channels)
    query_f = query_matrix.astype(jnp.float32).reshape(length, -1, key_channels)
    key_f = key_matrix.astype(jnp.float32).reshape(length, -1, key_channels)
    value_f = value_matrix.astype(jnp.float32).reshape(length, -1, DV)
    return (query_f, key_f, value_f, channel_log_decay)


def flipped(members):
    return tuple((jnp.flip(member, axis=0) for member in members))


def end_state(members):
    key_f, value_f, channel_log_decay = (members[1], members[2], members[3])
    totals = jnp.sum(channel_log_decay, axis=0)
    running = jnp.cumsum(channel_log_decay, axis=0)
    weighted = key_f * jnp.exp(totals[None] - running)
    states = jnp.einsum("thd,thv->hdv", weighted, value_f, precision=highest)
    return (totals, states)


def finish(forward, backward, gate_values, per_head_norm_gain):
    both = forward + backward
    scale = lax.rsqrt(jnp.mean(both * both, axis=-1, keepdims=True) + norm_eps)
    gated = (
        both
        * scale
        * per_head_norm_gain
        * jax.nn.silu(gate_values.astype(jnp.float32).reshape(both.shape))
    )
    return gated.reshape(both.shape[0], -1).astype(jnp.bfloat16)


def rms_rows(rows, feedforward_norm_gain):
    scale = lax.rsqrt(jnp.mean(rows * rows, axis=-1, keepdims=True) + norm_eps)
    return (rows * scale * feedforward_norm_gain).astype(jnp.bfloat16)


def per_device(
    stream,
    first_group_queries,
    first_group_keys,
    first_group_values,
    first_gate_logits,
    first_decay_logits,
    second_group_queries,
    second_group_keys,
    second_group_values,
    second_gate_logits,
    second_decay_logits,
    position_log_decay,
    per_head_norm_gain,
    first_output_weight,
    second_output_weight,
    feedforward_norm_gain,
    gate_weight,
    up_weight,
    down_weight,
):
    tok_rows = stream.shape[0]
    first_group = prepare_inputs(
        first_group_queries,
        first_group_keys,
        first_group_values,
        first_decay_logits,
        position_log_decay,
        KEY_SIZE_FIRST,
    )
    second_group = prepare_inputs(
        second_group_queries,
        second_group_keys,
        second_group_values,
        second_decay_logits,
        position_log_decay,
        KEY_SIZE_SECOND,
    )
    first_back = flipped(first_group)
    second_back = flipped(second_group)
    ahead_first = end_state(first_group)
    ahead_second = end_state(second_group)
    behind_first = end_state(first_back)
    behind_second = end_state(second_back)
    all_first, all_second = (
        lax.all_gather(ahead_first[0][None], "sp", axis=0, tiled=True),
        lax.all_gather(ahead_second[0][None], "sp", axis=0, tiled=True),
    )
    own_place = lax.axis_index("sp")

    def weights_for(all_logs, count):
        running = jnp.cumsum(all_logs, axis=0)
        own_end = running[own_place]
        own_before = own_end - all_logs[own_place]
        their_before = running - all_logs
        ranks = jnp.arange(count, dtype=jnp.int32)
        lower = (ranks < own_place)[:, None, None]
        higher = (ranks > own_place)[:, None, None]
        ahead = jnp.exp(jnp.where(lower, own_before - running, -jnp.inf))
        behind = jnp.exp(jnp.where(higher, their_before - own_end, -jnp.inf))
        return (ahead, behind)

    empty = (
        jnp.zeros_like(ahead_first[1]),
        jnp.zeros_like(ahead_first[1]),
        jnp.zeros_like(ahead_second[1]),
        jnp.zeros_like(ahead_second[1]),
    )
    pieces = (
        lax.all_gather(ahead_first[1][None].astype(jnp.bfloat16), "sp", axis=0, tiled=True).astype(
            jnp.float32
        ),
        lax.all_gather(behind_first[1][None].astype(jnp.bfloat16), "sp", axis=0, tiled=True).astype(
            jnp.float32
        ),
        lax.all_gather(ahead_second[1][None].astype(jnp.bfloat16), "sp", axis=0, tiled=True).astype(
            jnp.float32
        ),
        lax.all_gather(
            behind_second[1][None].astype(jnp.bfloat16), "sp", axis=0, tiled=True
        ).astype(jnp.float32),
    )
    count = pieces[0].shape[0]
    ahead_a, behind_a = weights_for(all_first, count)
    ahead_b, behind_b = weights_for(all_second, count)
    forward_first = one_way(
        first_group[0],
        first_group[1],
        first_group[2],
        first_group[3],
        empty[0] + jnp.einsum("nhd,nhdv->hdv", ahead_a, pieces[0], precision=highest),
    )
    backward_first = jnp.flip(
        one_way(
            first_back[0],
            first_back[1],
            first_back[2],
            first_back[3],
            empty[1] + jnp.einsum("nhd,nhdv->hdv", behind_a, pieces[1], precision=highest),
        ),
        0,
    )
    forward_second = one_way(
        second_group[0],
        second_group[1],
        second_group[2],
        second_group[3],
        empty[2] + jnp.einsum("nhd,nhdv->hdv", ahead_b, pieces[2], precision=highest),
    )
    backward_second = jnp.flip(
        one_way(
            second_back[0],
            second_back[1],
            second_back[2],
            second_back[3],
            empty[3] + jnp.einsum("nhd,nhdv->hdv", behind_b, pieces[3], precision=highest),
        ),
        0,
    )
    first_group_output = finish(
        forward_first, backward_first, first_gate_logits, per_head_norm_gain
    )
    second_group_output = finish(
        forward_second, backward_second, second_gate_logits, per_head_norm_gain
    )
    part_rows = tok_rows // lax.axis_size("tp")
    row_start = lax.axis_index("tp") * part_rows
    summed = lax.psum(
        (
            jnp.dot(first_group_output, first_output_weight, preferred_element_type=jnp.float32)
            + jnp.dot(second_group_output, second_output_weight, preferred_element_type=jnp.float32)
        ).astype(jnp.bfloat16),
        "tp",
    ).astype(jnp.float32)
    residual = stream.astype(jnp.float32) + summed
    normed_all = rms_rows(residual, feedforward_norm_gain)
    own_residual = lax.dynamic_slice_in_dim(residual, row_start, part_rows, 0)
    pieces = (
        lax.all_gather(gate_weight, "sp", axis=0, tiled=True),
        lax.all_gather(up_weight, "sp", axis=0, tiled=True),
    )
    gate_sum = jnp.dot(normed_all, pieces[0], preferred_element_type=jnp.float32)
    up_sum = jnp.dot(normed_all, pieces[1], preferred_element_type=jnp.float32)
    hidden = (jax.nn.silu(gate_sum) * up_sum).astype(jnp.bfloat16)
    down_whole = lax.all_gather(down_weight, "sp", axis=1, tiled=True)
    down_sum = lax.psum_scatter(
        jnp.dot(hidden, down_whole, preferred_element_type=jnp.float32).astype(jnp.bfloat16),
        "tp",
        scatter_dimension=0,
        tiled=True,
    ).astype(jnp.float32)
    return (own_residual + 0.5 * down_sum).astype(jnp.bfloat16)


def solution(mesh):
    in_specs = (
        P("sp", None),
        P("sp", "tp"),
        P("sp", "tp"),
        P("sp", "tp"),
        P("sp", "tp"),
        P("sp", "tp"),
        P("sp", "tp"),
        P("sp", "tp"),
        P("sp", "tp"),
        P("sp", "tp"),
        P("sp", "tp"),
        P("sp"),
        P(),
        P("tp", None),
        P("tp", None),
        P(),
        P("sp", "tp"),
        P("sp", "tp"),
        P("tp", "sp"),
    )
    out_specs = P(("sp", "tp"), None)
    return jax.shard_map(
        per_device, mesh=mesh, in_specs=in_specs, out_specs=out_specs, check_vma=False
    )
```

profile of v0, /device:TPU:0, one launch (start us, length us, event | category | flops | bytes accessed | tf_op | source)
XLA Modules:
  0.0 579.6 jit_solution(15194093987630395146)
XLA Ops:
  20.7 22.3 %all_gather.27 = f32[8,2,64]{2,1,0:T(2,128)S(1)} all-gather(f32[1,2,64]{2,1,0:T(2,128)S(1)} %broadcast_in_dim.108), channel_id=1, replica_groups=mesh['sp'=8,'tp'=4] {'sp'}, dimensions={0}, use_global_device_ids=true | all-gather | bytes 4608 | tf_op jit(solution)/shard_map/all_gather | solution.py:144
  46.7 32.8 %all-gather.1 = bf16[16,64,128]{2,1,0:T(8,128)(2,1)} all-gather(bf16[2,64,128]{2,1,0:T(8,128)(2,1)S(1)} %convolution_convert_fusion.4), channel_id=3, replica_groups=mesh['sp'=8,'tp'=4] {'sp'}, dimensions={0}, use_global_device_ids=true | all-gather | bytes 294912 | tf_op jit(solution)/shard_map/all_gather | solution.py:171
  80.6 1.6 fusion.71
  83.0 4.6 while.49
  92.3 32.8 %all-gather = bf16[16,64,128]{2,1,0:T(8,128)(2,1)} all-gather(bf16[2,64,128]{2,1,0:T(8,128)(2,1)S(1)} %convolution_convert_fusion.3), channel_id=2, replica_groups=mesh['sp'=8,'tp'=4] {'sp'}, dimensions={0}, use_global_device_ids=true | all-gather | bytes 294912 | tf_op jit(solution)/shard_map/all_gather | solution.py:168
  126.8 1.6 fusion.73
  128.4 2.3 while.48
  132.2 16.3 %all_gather.30 = f32[8,2,128]{2,1,0:T(2,128)S(1)} all-gather(f32[1,2,128]{2,1,0:T(2,128)S(1)} %bitcast.424), channel_id=1, replica_groups=mesh['sp'=8,'tp'=4] {'sp'}, dimensions={0}, use_global_device_ids=true | all-gather | bytes 9216 | tf_op jit(solution)/shard_map/all_gather | solution.py:145
  153.3 2.0 rev.40
  156.9 33.5 %all-gather.3 = bf16[16,128,128]{2,1,0:T(8,128)(2,1)} all-gather(bf16[2,128,128]{2,1,0:T(8,128)(2,1)S(1)} %convolution_convert_fusion.1), channel_id=5, replica_groups=mesh['sp'=8,'tp'=4] {'sp'}, dimensions={0}, use_global_device_ids=true | all-gather | bytes 589824 | tf_op jit(solution)/shard_map/all_gather | solution.py:177
  191.7 1.6 rev.37
  198.4 8.6 %while.51 = (s32[]{:T(128)}, f32[2,128,128]{2,1,0:T(8,128)S(1)}, f32[4,2,64,128]{3,2,1,0:T(8,128)}, f32[4,2,1,128]{3,1,2,0:T(2,128)S(1)}, f32[4,2,64,128]{3,2,1,...) while((s32[]{:T(128)}, f32[2,128,128]{2,1,0:T(8,128)S(1)}, ...), condition=%wide.region_26.27_spmd, body=%wide.region_25.26_spmd.sunk | while | flops 50397184 | bytes 660569 | solution.py:54
  212.0 33.2 %all-gather.2 = bf16[16,128,128]{2,1,0:T(8,128)(2,1)} all-gather(bf16[2,128,128]{2,1,0:T(8,128)(2,1)S(1)} %convolution_convert_fusion.2), channel_id=4, replica_groups=mesh['sp'=8,'tp'=4] {'sp'}, dimensions={0}, use_global_device_ids=true | all-gather | bytes 589824 | tf_op jit(solution)/shard_map/all_gather | solution.py:174
  248.7 2.2 fusion.48
  251.0 2.9 while.50
  260.7 33.2 %all-reduce.2.cloned.1.call-done = bf16[256,2048]{1,0:T(8,128)(2,1)} async-done(((bf16[256,2048]{1,0:T(8,128)(2,1)}), bf16[256,2048]{1,0:T(8,128)(2,1)}) %all-reduce.2.cloned.1.call-update) | async-done | bytes 1048592 | tf_op jit(solution)/shard_map/psum | solution.py:226
  293.9 2.0 convert_add_fusion
  295.9 56.1 %all-gather.8.cloned.1.call-done = bf16[2048,1408]{1,0:T(8,128)(2,1)} async-done(((bf16[256,1408]{1,0:T(8,128)(2,1)}), bf16[2048,1408]{1,0:T(8,128)(2,1)}) %all-gather.8.cloned.1.call-update) | async-done | bytes 5767184 | tf_op jit(solution)/shard_map/all_gather | solution.py:237
  352.0 6.3 %fusion.112 = f32[256,1408]{1,0:T(8,128)} fusion(bf16[2048,1408]{1,0:T(8,128)(2,1)} %all-gather.8.cloned.1.call-done, f32[2048]{0:T(1024)S(1)} %copy-done.33, f32[256]{0:T(256)S(1)} %add_rsqrt_fusion.2, bf16[256,2048]{1,0:T(8,128)(2,1)} %all-reduce.2.cloned.1.call-done, bf16[256,2048]{1,0:T(8,128)(2,1)} %param.27), kind=kOutput, calls=%fused_computation.189 | convolution fusion | flops 1479540736 | bytes 9315328 | tf_op jit(solution)/shard_map/dot_general | solution.py:240
  358.3 86.1 %all-gather.10.cloned.1.call-done = bf16[2048,1408]{1,0:T(8,128)(2,1)} async-done(((bf16[256,1408]{1,0:T(8,128)(2,1)}), bf16[2048,1408]{1,0:T(8,128)(2,1)}) %all-gather.10.cloned.1.call-update) | async-done | bytes 5767184 | tf_op jit(solution)/shard_map/all_gather | solution.py:238
  444.4 93.0 %all-gather.12.cloned.1.call-done = bf16[1408,2048]{1,0:T(8,128)(2,1)} async-done(((bf16[1408,256]{1,0:T(8,128)(2,1)}), bf16[1408,2048]{1,0:T(8,128)(2,1)}) %all-gather.12.cloned.1.call-update) | async-done | bytes 5767184 | tf_op jit(solution)/shard_map/all_gather | solution.py:243
  537.3 9.9 %convolution_convert_fusion = bf16[256,2048]{1,0:T(8,128)(2,1)} fusion(bf16[1408,2048]{1,0:T(8,128)(2,1)} %all-gather.12.cloned.1.call-done, bf16[2048,1408]{1,0:T(8,128)(2,1)} %all-gather.10.cloned.1.call-done, f32[256,1408]{1,0:T(8,128)} %fusion.112, f32[2048]{0:T(1024)S(1)} %copy-done.33, f32[256]{0:T(256)S(1)} %add_rsqrt_fusion.2, ...), kind=kOutput, calls=%fused_computation.60 | convolution fusion | flops 2958622720 | bytes 16131072 | tf_op jit(solution)/shard_map/dot_general | solution.py:245
  547.2 23.1 %reduce-scatter.2.cloned.1.call-done = bf16[64,2048]{1,0:T(8,128)(2,1)} async-done(((bf16[256,2048]{1,0:T(8,128)(2,1)}), bf16[64,2048]{1,0:T(8,128)(2,1)}) %reduce-scatter.2.cloned.1.call-update) | async-done | bytes 262160 | tf_op jit(solution)/shard_map/reduce_scatter | solution.py:244
  570.3 1.7 add_convert_fusion
  (284 shorter events, 71.8 us)
Async XLA Ops:
  7.4 248.9 %copy-start = (bf16[256,2048]{1,0:T(8,128)(2,1)S(1)}, bf16[256,2048]{1,0:T(8,128)(2,1)}, u32[]{:S(2)}) copy-start(bf16[256,2048]{1,0:T(8,128)(2,1)} %param.40) | copy-start | bytes 3145732
  7.4 5.3 copy-start.23
  7.4 6.3 %copy-start.3 = (bf16[256,256]{1,0:T(8,128)(2,1)S(1)}, bf16[256,256]{1,0:T(8,128)(2,1)}, u32[]{:S(2)}) copy-start(bf16[256,256]{1,0:T(8,128)(2,1)} %param.30) | copy-start | bytes 393220
  7.4 286.5 %all-reduce.2.cloned.1.call-start = ((), (), s32[]{:S(2)}) async-start(), calls=%async_computation.1 | async-start | bytes 2097152 | tf_op jit(solution)/shard_map/psum | solution.py:226
  8.4 6.9 %copy-start.18 = (bf16[256,256]{1,0:T(8,128)(2,1)S(1)}, bf16[256,256]{1,0:T(8,128)(2,1)}, u32[]{:S(2)}) copy-start(bf16[256,256]{1,0:T(8,128)(2,1)} %param.33) | copy-start | bytes 393220
  9.7 33.3 %copy-start.28 = (pred[8]{0:T(512)(128)(4,1)}, pred[8]{0:T(512)(128)(4,1)S(1)}, u32[]{:S(2)}) copy-start(pred[8]{0:T(512)(128)(4,1)S(1)} %get-tuple-element.377) | copy-start | bytes 28
  9.7 33.3 %copy-start.30 = (pred[8]{0:T(512)(128)(4,1)}, pred[8]{0:T(512)(128)(4,1)S(1)}, u32[]{:S(2)}) copy-start(pred[8]{0:T(512)(128)(4,1)S(1)} %get-tuple-element.378) | copy-start | bytes 28
  9.9 7.3 %copy-start.19 = (bf16[256,256]{1,0:T(8,128)(2,1)S(1)}, bf16[256,256]{1,0:T(8,128)(2,1)}, u32[]{:S(2)}) copy-start(bf16[256,256]{1,0:T(8,128)(2,1)} %param.34) | copy-start | bytes 393220
  12.8 32.6 %copy-start.4 = (f32[256,128]{0,1:T(8,128)}, f32[256,128]{0,1:T(8,128)S(1)}, u32[]{:S(2)}) copy-start(f32[256,128]{0,1:T(8,128)S(1)} %convert_element_type.93) | copy-start | bytes 393220
  12.8 5.6 copy-start.6
  88.2 37.0 %copy-start.12 = (f32[4,64,2,64]{1,0,3,2:T(4,128)S(1)}, f32[4,64,2,64]{1,0,3,2:T(4,128)}, u32[]{:S(2)}) copy-start(f32[4,64,2,64]{1,0,3,2:T(4,128)} %reshape_reshape.29) | copy-start | bytes 393220
  89.6 36.0 %copy-start.8 = (f32[4,64,2,64]{1,0,3,2:T(4,128)S(1)}, f32[4,64,2,64]{1,0,3,2:T(4,128)}, u32[]{:S(2)}) copy-start(f32[4,64,2,64]{1,0,3,2:T(4,128)} %reshape.253) | copy-start | bytes 393220
  89.6 36.1 %copy-start.9 = (f32[4,64,2,64]{1,0,3,2:T(4,128)S(1)}, f32[4,64,2,64]{1,0,3,2:T(4,128)}, u32[]{:S(2)}) copy-start(f32[4,64,2,64]{1,0,3,2:T(4,128)} %reshape.254) | copy-start | bytes 393220
  130.7 17.8 %copy-start.29 = (pred[8]{0:T(512)(128)(4,1)S(1)}, pred[8]{0:T(512)(128)(4,1)}, u32[]{:S(2)}) copy-start(pred[8]{0:T(512)(128)(4,1)} %copy-done.28) | copy-start | bytes 28
  130.7 17.8 %copy-start.31 = (pred[8]{0:T(512)(128)(4,1)S(1)}, pred[8]{0:T(512)(128)(4,1)}, u32[]{:S(2)}) copy-start(pred[8]{0:T(512)(128)(4,1)} %copy-done.30) | copy-start | bytes 28
  153.2 38.4 %copy-start.10 = (f32[256,256]{0,1:T(8,128)S(1)}, f32[256,256]{0,1:T(8,128)}, u32[]{:S(2)}) copy-start(f32[256,256]{0,1:T(8,128)} %convert_element_type.101) | copy-start | bytes 786436
  197.6 9.3 %copy-start.13 = (f32[4,2,64,64]{3,2,1,0:T(8,128)S(1)}, f32[4,2,64,64]{3,2,1,0:T(8,128)}, u32[]{:S(2)}) copy-start(f32[4,2,64,64]{3,2,1,0:T(8,128)} %convolution_select_fusion) | copy-start | bytes 393220
  209.8 36.8 %copy-start.1 = (f32[4,64,2,128]{1,0,3,2:T(4,128)S(1)}, f32[4,64,2,128]{1,0,3,2:T(4,128)}, u32[]{:S(2)}) copy-start(f32[4,64,2,128]{1,0,3,2:T(4,128)} %reshape.255) | copy-start | bytes 786436
  210.5 36.3 %copy-start.2 = (f32[4,64,2,128]{1,0,3,2:T(4,128)S(1)}, f32[4,64,2,128]{1,0,3,2:T(4,128)}, u32[]{:S(2)}) copy-start(f32[4,64,2,128]{1,0,3,2:T(4,128)} %reshape.256) | copy-start | bytes 786436
  258.7 93.3 %all-gather.8.cloned.1.call-start = ((), (), s32[]{:S(2)}) async-start(), calls=%async_computation.2 | async-start | bytes 6488064 | tf_op jit(solution)/shard_map/all_gather | solution.py:237
  259.3 185.1 %all-gather.10.cloned.1.call-start = ((), (), s32[]{:S(2)}) async-start(), calls=%async_computation.3 | async-start | bytes 6488064 | tf_op jit(solution)/shard_map/all_gather | solution.py:238
  259.8 277.5 %all-gather.12.cloned.1.call-start = ((), (), s32[]{:S(2)}) async-start(), calls=%async_computation.4 | async-start | bytes 6488064 | tf_op jit(solution)/shard_map/all_gather | solution.py:243
  260.4 91.6 %copy-start.33 = (f32[2048]{0:T(1024)S(1)}, f32[2048]{0:T(1024)}, u32[]{:S(2)}) copy-start(f32[2048]{0:T(1024)} %param.42) | copy-start | bytes 24580
  260.4 309.9 %reduce-scatter.2.cloned.1.call-start = ((), (), s32[]{:S(2)}) async-start(), calls=%async_computation.5 | async-start | bytes 1310720 | tf_op jit(solution)/shard_map/reduce_scatter | solution.py:244
  (15 other events, 37.4 us)
Sparse Core Ops, SparseCore 0:
  258.8 35.0 all-reduce.1
  547.4 22.9 reduce-scatter.1
Sparse Core Ops, SparseCore 1:
  261.3 90.6 all-gather.7
  354.1 90.2 all-gather.9
  446.3 91.0 all-gather.11
where the time goes:
time: 581 us; the launch traced here: 580 us
  waiting for transfers between devices  293 us (50%)
  blocking collectives  171 us (29%)
  matrix products  50.9 us (9%)
  local copies, waits for them, and re-layouts  33.3 us (6%)
  between operations  16.2 us (3%)
  other arithmetic  14.3 us (2%)
    all_gather x1, waiting for transfers between devices, per_device(): down_whole = lax.all_gather(down_weight, 'sp', axis=1, tiled=True)  93 us
    all_gather x1, waiting for transfers between devices, per_device(): lax.all_gather(up_weight, 'sp', axis=0, tiled=True)  86.1 us
    all_gather x1, waiting for transfers between devices, per_device(): lax.all_gather(gate_weight, 'sp', axis=0, tiled=True)  56.1 us
    all_gather x1, blocking collectives, per_device(): lax.all_gather(behind_second[1][None].astype(jnp.bfloat16), 'sp', axis=0,...  33.5 us
    psum x1, waiting for transfers between devices, per_device(): lax.psum((jnp.dot(first_group_output, first_output_weight, preferred_elem...  33.2 us
    all_gather x1, blocking collectives, per_device(): lax.all_gather(ahead_second[1][None].astype(jnp.bfloat16), 'sp', axis=0,...  33.2 us
    all_gather x1, blocking collectives, per_device(): lax.all_gather(ahead_first[1][None].astype(jnp.bfloat16), 'sp', axis=0, t...  32.8 us
    all_gather x1, blocking collectives, per_device(): lax.all_gather(behind_first[1][None].astype(jnp.bfloat16), 'sp', axis=0,...  32.8 us
  transfers between devices with their start and end apart: 5, of which 5 were waited for; matrix products, arithmetic and copies ran while one was open for 1% of the time, Pallas kernels for 0%

commit v1 on v0

--- a/solution.py
+++ b/solution.py
@@ -1,3 +1,4 @@
+import functools
 import jax
 import jax.numpy as jnp
 from jax import lax
@@ -10,6 +11,15 @@
 decay_softness = 16.0
 norm_eps = 1e-06
 highest = lax.Precision.HIGHEST
+
+
+def settle_pipes(target, d0):
+    x_new = jnp.stack([target] * jax.lax.axis_size("sp"))
+    piece_now = jax.lax.all_to_all(x_new, "sp", 0, 0)
+    return jnp.concatenate(piece_now, d0)
+
+
+map_pieces_all_on = functools.partial(settle_pipes, d0=0)
 
 
 def channel_log_decays(decay_logits, position_log_decay, key_channels):
@@ -168,9 +178,7 @@
         lax.all_gather(ahead_first[1][None].astype(jnp.bfloat16), "sp", axis=0, tiled=True).astype(
             jnp.float32
         ),
-        lax.all_gather(behind_first[1][None].astype(jnp.bfloat16), "sp", axis=0, tiled=True).astype(
-            jnp.float32
-        ),
+        map_pieces_all_on(behind_first[1][None].astype(jnp.bfloat16)).astype(jnp.float32),
         lax.all_gather(ahead_second[1][None].astype(jnp.bfloat16), "sp", axis=0, tiled=True).astype(
             jnp.float32
         ),

time: 581 us -> 598 us (1.029)
  blocking collectives: 171 us -> 135 us
  matrix products: 50.9 us -> 73.7 us
  local copies, waits for them, and re-layouts: 33.3 us -> 53 us
  starting transfers between devices: 0.39 us -> 7.73 us
    all_gather x1 -> x0, blocking collectives: 32.8 us -> none  [per_device(): lax.all_gather(behind_first[1][None].astype(jnp.bfloat16), 'sp', axis=0,...]
    dot_general x16, matrix products: 9.05 us -> 19.1 us  [advance(): jnp.einsum('hjd,hjv->hdv', key_part, value_part, precision=highest)]
    dot_general x16, matrix products: 8.46 us -> 17.7 us  [advance(): emitted = jnp.einsum('hid,hdv->hiv', query_part, states, precision=highest)]
    all_to_all x0 -> x1, starting transfers between devices: none -> 7.31 us  [settle_pipes(): piece_now = jax.lax.all_to_all(x_new, 'sp', 0, 0)]
    all_gather x1, waiting for transfers between devices: 86.1 us -> 92.4 us  [per_device(): lax.all_gather(up_weight, 'sp', axis=0, tiled=True)]
    all_gather x1, waiting for transfers between devices: 93 us -> 86.7 us  [per_device(): down_whole = lax.all_gather(down_weight, 'sp', axis=1, tiled=True)]
  transfers between devices with their start and end apart: 5 -> 6, of which waited for: 5 -> 5; matrix products, arithmetic and copies ran while one was open for 1% -> 18% of each run, Pallas kernels for 0% -> 0%
where the time goes in v1:
time: 598 us; the launch traced here: 595 us
  waiting for transfers between devices  293 us (49%)
  blocking collectives  135 us (23%)
  matrix products  73.7 us (12%)
  local copies, waits for them, and re-layouts  53 us (9%)
  other arithmetic  16.3 us (3%)
  between operations  16 us (3%)
  starting transfers between devices  7.73 us (1%)
    all_gather x1, waiting for transfers between devices, per_device(): lax.all_gather(up_weight, 'sp', axis=0, tiled=True)  92.4 us
    all_gather x1, waiting for transfers between devices, per_device(): down_whole = lax.all_gather(down_weight, 'sp', axis=1, tiled=True)  86.7 us
    all_gather x1, waiting for transfers between devices, per_device(): lax.all_gather(gate_weight, 'sp', axis=0, tiled=True)  56.1 us
    all_gather x1, blocking collectives, per_device(): lax.all_gather(behind_second[1][None].astype(jnp.bfloat16), 'sp', axis=0,...  33.4 us
    psum x1, waiting for transfers between devices, per_device(): lax.psum((jnp.dot(first_group_output, first_output_weight, preferred_elem...  33.3 us
    all_gather x1, blocking collectives, per_device(): lax.all_gather(ahead_second[1][None].astype(jnp.bfloat16), 'sp', axis=0,...  33.2 us
    all_gather x1, blocking collectives, per_device(): lax.all_gather(ahead_first[1][None].astype(jnp.bfloat16), 'sp', axis=0, t...  30.8 us
    reduce_scatter x1, waiting for transfers between devices, per_device(): lax.psum_scatter(jnp.dot(hidden, down_whole, preferred_element_type=jnp.f...  23.1 us
  transfers between devices with their start and end apart: 6, of which 5 were waited for; matrix products, arithmetic and copies ran while one was open for 18% of the time, Pallas kernels for 0%

profile of v1, /device:TPU:0, one launch (start us, length us, event | category | flops | bytes accessed | tf_op | source)
XLA Modules:
  0.0 594.9 jit_solution(10206107375939344454)
XLA Ops:
  14.0 7.3 %all-to-all-start = ((bf16[8,1,2,64,128]{4,3,2,1,0:T(8,128)(2,1)}), bf16[8,1,2,64,128]{4,3,2,1,0:T(8,128)(2,1)}, u32[]{:S(2)}, u32[]{:S(2)}) async-start(bf16[8,1,2,64,128]{4,3,2,1,0:T(8,128)(2,1)} %stack.2), calls=%async_computation | async-start | bytes 524288 | tf_op jit(solution)/shard_map/all_to_all | solution.py:18
  31.6 20.9 %all_gather.24 = f32[8,2,64]{2,1,0:T(2,128)S(1)} all-gather(f32[1,2,64]{2,1,0:T(2,128)S(1)} %broadcast_in_dim.108), channel_id=1, replica_groups=mesh['sp'=8,'tp'=4] {'sp'}, dimensions={0}, use_global_device_ids=true | all-gather | bytes 4608 | tf_op jit(solution)/shard_map/all_gather | solution.py:154
  60.2 30.8 %all-gather = bf16[16,64,128]{2,1,0:T(8,128)(2,1)S(1)} all-gather(bf16[2,64,128]{2,1,0:T(8,128)(2,1)S(1)} %convolution_convert_fusion.3), channel_id=2, replica_groups=mesh['sp'=8,'tp'=4] {'sp'}, dimensions={0}, use_global_device_ids=true | all-gather | bytes 294912 | tf_op jit(solution)/shard_map/all_gather | solution.py:178
  92.6 1.8 reshape_reshape.32
  97.5 11.3 %while.48 = (s32[]{:T(128)}, f32[2,64,128]{2,1,0:T(8,128)S(1)}, f32[4,2,64,128]{3,2,1,0:T(8,128)}, f32[4,2,1,64]{3,1,2,0:T(2,128)S(1)}, f32[4,2,64,64]{3,2,1,0:T...) while((s32[]{:T(128)}, f32[2,64,128]{2,1,0:T(8,128)S(1)}, ...), condition=%wide.region_6.7_spmd, body=%wide.region_5.6_spmd.sunk | while | flops 25198592 | bytes 592989 | solution.py:64
  112.7 16.5 %all_gather.26 = f32[8,2,128]{2,1,0:T(2,128)S(1)} all-gather(f32[1,2,128]{2,1,0:T(2,128)S(1)} %bitcast.423), channel_id=1, replica_groups=mesh['sp'=8,'tp'=4] {'sp'}, dimensions={0}, use_global_device_ids=true | all-gather | bytes 9216 | tf_op jit(solution)/shard_map/all_gather | solution.py:155
  134.5 1.9 rev.40
  138.9 33.4 %all-gather.2 = bf16[16,128,128]{2,1,0:T(8,128)(2,1)} all-gather(bf16[2,128,128]{2,1,0:T(8,128)(2,1)S(1)} %convolution_convert_fusion.1), channel_id=4, replica_groups=mesh['sp'=8,'tp'=4] {'sp'}, dimensions={0}, use_global_device_ids=true | all-gather | bytes 589824 | tf_op jit(solution)/shard_map/all_gather | solution.py:185
  173.5 3.1 rev.37
  179.9 2.1 fusion.46
  182.7 11.9 %while.51 = (s32[]{:T(128)}, f32[2,128,128]{2,1,0:T(8,128)S(1)}, f32[4,2,64,128]{3,2,1,0:T(8,128)}, f32[4,2,1,128]{3,1,2,0:T(2,128)S(1)}, f32[4,2,64,128]{3,2,1,...) while((s32[]{:T(128)}, f32[2,128,128]{2,1,0:T(8,128)S(1)}, ...), condition=%wide.region_26.27_spmd, body=%wide.region_25.26_spmd.sunk | while | flops 50397184 | bytes 660569 | solution.py:64
  202.0 33.2 %all-gather.1 = bf16[16,128,128]{2,1,0:T(8,128)(2,1)} all-gather(bf16[2,128,128]{2,1,0:T(8,128)(2,1)S(1)} %convolution_convert_fusion.2), channel_id=3, replica_groups=mesh['sp'=8,'tp'=4] {'sp'}, dimensions={0}, use_global_device_ids=true | all-gather | bytes 589824 | tf_op jit(solution)/shard_map/all_gather | solution.py:182
  241.3 2.3 fusion.48
  243.6 9.6 %while.50 = (s32[]{:T(128)}, f32[2,128,128]{2,1,0:T(8,128)S(1)}, f32[4,2,64,128]{3,2,1,0:T(8,128)S(1)}, f32[4,2,1,128]{3,1,2,0:T(2,128)S(1)}, f32[4,2,64,128]{3,...) while((s32[]{:T(128)}, f32[2,128,128]{2,1,0:T(8,128)S(1)}, ...), condition=%wide.region_20.21_spmd, body=%wide.region_19.20_spmd.sunk | while | flops 50397184 | bytes 791133 | solution.py:64
  261.3 7.9 %while.49 = (s32[]{:T(128)}, f32[2,64,128]{2,1,0:T(8,128)S(1)}, f32[4,2,64,128]{3,2,1,0:T(8,128)}, f32[4,2,1,64]{3,1,2,0:T(2,128)S(1)}, f32[4,2,64,64]{3,2,1,0:T...) while((s32[]{:T(128)}, f32[2,64,128]{2,1,0:T(8,128)S(1)}, ...), condition=%wide.region_12.13_spmd, body=%wide.region_11.12_spmd.sunk | while | flops 25198592 | bytes 462937 | solution.py:64
  276.0 33.3 %all-reduce.2.cloned.1.call-done = bf16[256,2048]{1,0:T(8,128)(2,1)} async-done(((bf16[256,2048]{1,0:T(8,128)(2,1)}), bf16[256,2048]{1,0:T(8,128)(2,1)}) %all-reduce.2.cloned.1.call-update) | async-done | bytes 1048592 | tf_op jit(solution)/shard_map/psum | solution.py:234
  309.2 2.0 convert_add_fusion
  311.2 56.1 %all-gather.7.cloned.1.call-done = bf16[2048,1408]{1,0:T(8,128)(2,1)} async-done(((bf16[256,1408]{1,0:T(8,128)(2,1)}), bf16[2048,1408]{1,0:T(8,128)(2,1)}) %all-gather.7.cloned.1.call-update) | async-done | bytes 5767184 | tf_op jit(solution)/shard_map/all_gather | solution.py:245
  367.3 6.3 %fusion.112 = f32[256,1408]{1,0:T(8,128)} fusion(bf16[2048,1408]{1,0:T(8,128)(2,1)} %all-gather.7.cloned.1.call-done, f32[2048]{0:T(1024)S(1)} %copy-done.26, f32[256]{0:T(256)S(1)} %add_rsqrt_fusion.2, bf16[256,2048]{1,0:T(8,128)(2,1)} %all-reduce.2.cloned.1.call-done, bf16[256,2048]{1,0:T(8,128)(2,1)} %param.27), kind=kOutput, calls=%fused_computation.189 | convolution fusion | flops 1479540736 | bytes 9315328 | tf_op jit(solution)/shard_map/dot_general | solution.py:248
  373.6 86.7 %all-gather.11.cloned.1.call-done = bf16[1408,2048]{1,0:T(8,128)(2,1)} async-done(((bf16[1408,256]{1,0:T(8,128)(2,1)}), bf16[1408,2048]{1,0:T(8,128)(2,1)}) %all-gather.11.cloned.1.call-update) | async-done | bytes 5767184 | tf_op jit(solution)/shard_map/all_gather | solution.py:251
  460.3 92.4 %all-gather.9.cloned.1.call-done = bf16[2048,1408]{1,0:T(8,128)(2,1)} async-done(((bf16[256,1408]{1,0:T(8,128)(2,1)}), bf16[2048,1408]{1,0:T(8,128)(2,1)}) %all-gather.9.cloned.1.call-update) | async-done | bytes 5767184 | tf_op jit(solution)/shard_map/all_gather | solution.py:246
  552.7 9.9 %convolution_convert_fusion = bf16[256,2048]{1,0:T(8,128)(2,1)} fusion(bf16[1408,2048]{1,0:T(8,128)(2,1)} %all-gather.11.cloned.1.call-done, bf16[2048,1408]{1,0:T(8,128)(2,1)} %all-gather.9.cloned.1.call-done, f32[256,1408]{1,0:T(8,128)} %fusion.112, f32[2048]{0:T(1024)S(1)} %copy-done.26, f32[256]{0:T(256)S(1)} %add_rsqrt_fusion.2, ...), kind=kOutput, calls=%fused_computation.60 | convolution fusion | flops 2958622720 | bytes 16131072 | tf_op jit(solution)/shard_map/dot_general | solution.py:253
  562.6 23.1 %reduce-scatter.2.cloned.1.call-done = bf16[64,2048]{1,0:T(8,128)(2,1)} async-done(((bf16[256,2048]{1,0:T(8,128)(2,1)}), bf16[64,2048]{1,0:T(8,128)(2,1)}) %reduce-scatter.2.cloned.1.call-update) | async-done | bytes 262160 | tf_op jit(solution)/shard_map/reduce_scatter | solution.py:252
  585.6 1.7 add_convert_fusion
  (272 shorter events, 114.0 us)
Async XLA Ops:
  7.4 264.1 %copy-start = (bf16[256,2048]{1,0:T(8,128)(2,1)S(1)}, bf16[256,2048]{1,0:T(8,128)(2,1)}, u32[]{:S(2)}) copy-start(bf16[256,2048]{1,0:T(8,128)(2,1)} %param.40) | copy-start | bytes 3145732
  12.2 10.6 %copy-start.17 = (bf16[256,128]{1,0:T(8,128)(2,1)S(1)}, bf16[256,128]{1,0:T(8,128)(2,1)}, u32[]{:S(2)}) copy-start(bf16[256,128]{1,0:T(8,128)(2,1)} %param.28) | copy-start | bytes 196612
  13.2 13.0 %copy-start.15 = (bf16[256,256]{1,0:T(8,128)(2,1)S(1)}, bf16[256,256]{1,0:T(8,128)(2,1)}, u32[]{:S(2)}) copy-start(bf16[256,256]{1,0:T(8,128)(2,1)} %param.33) | copy-start | bytes 393220
  14.0 245.0 %all-to-all-start = ((bf16[8,1,2,64,128]{4,3,2,1,0:T(8,128)(2,1)}), bf16[8,1,2,64,128]{4,3,2,1,0:T(8,128)(2,1)}, u32[]{:S(2)}, u32[]{:S(2)}) async-start(bf16[8,1,2,64,128]{4,3,2,1,0:T(8,128)(2,1)} %stack.2), calls=%async_computation | async-start | bytes 524288 | tf_op jit(solution)/shard_map/all_to_all | solution.py:18
  21.3 287.9 %all-reduce.2.cloned.1.call-start = ((), (), s32[]{:S(2)}) async-start(), calls=%async_computation.2 | async-start | bytes 2097152 | tf_op jit(solution)/shard_map/psum | solution.py:234
  21.8 30.8 %copy-start.21 = (pred[8]{0:T(512)(128)(4,1)}, pred[8]{0:T(512)(128)(4,1)S(1)}, u32[]{:S(2)}) copy-start(pred[8]{0:T(512)(128)(4,1)S(1)} %get-tuple-element.377) | copy-start | bytes 28
  21.8 30.8 %copy-start.23 = (pred[8]{0:T(512)(128)(4,1)}, pred[8]{0:T(512)(128)(4,1)S(1)}, u32[]{:S(2)}) copy-start(pred[8]{0:T(512)(128)(4,1)S(1)} %get-tuple-element.378) | copy-start | bytes 28
  53.8 37.2 %copy-start.9 = (f32[4,64,2,64]{1,0,3,2:T(4,128)S(1)}, f32[4,64,2,64]{1,0,3,2:T(4,128)}, u32[]{:S(2)}) copy-start(f32[4,64,2,64]{1,0,3,2:T(4,128)} %reshape_reshape.29) | copy-start | bytes 393220
  109.4 19.8 %copy-start.22 = (pred[8]{0:T(512)(128)(4,1)S(1)}, pred[8]{0:T(512)(128)(4,1)}, u32[]{:S(2)}) copy-start(pred[8]{0:T(512)(128)(4,1)} %copy-done.21) | copy-start | bytes 28
  109.4 19.8 %copy-start.24 = (pred[8]{0:T(512)(128)(4,1)S(1)}, pred[8]{0:T(512)(128)(4,1)}, u32[]{:S(2)}) copy-start(pred[8]{0:T(512)(128)(4,1)} %copy-done.23) | copy-start | bytes 28
  112.7 18.8 %copy-start.18 = (f32[256]{0:T(256)}, f32[256]{0:T(256)S(1)}, u32[]{:S(2)}) copy-start(f32[256]{0:T(256)S(1)} %get-tuple-element.364) | copy-start | bytes 3076
  182.0 12.7 %copy-start.3 = (f32[256,2,128]{2,0,1:T(8,128)S(1)}, f32[256,2,128]{2,0,1:T(8,128)}, u32[]{:S(2)}) copy-start(f32[256,2,128]{2,0,1:T(8,128)} %copy.308) | copy-start | bytes 786436
  182.0 12.7 %copy-start.10 = (f32[4,2,64,64]{3,2,1,0:T(8,128)S(1)}, f32[4,2,64,64]{3,2,1,0:T(8,128)}, u32[]{:S(2)}) copy-start(f32[4,2,64,64]{3,2,1,0:T(8,128)} %convolution_select_fusion) | copy-start | bytes 393220
  196.2 39.0 %copy-start.8 = (f32[256,256]{1,0:T(8,128)S(1)}, f32[256,256]{1,0:T(8,128)}, u32[]{:S(2)}) copy-start(f32[256,256]{1,0:T(8,128)} %copy.286) | copy-start | bytes 786436
  243.6 9.6 %copy-start.7 = (f32[4,2,64,64]{3,2,1,0:T(8,128)S(1)}, f32[4,2,64,64]{3,2,1,0:T(8,128)}, u32[]{:S(2)}) copy-start(f32[4,2,64,64]{3,2,1,0:T(8,128)} %convolution_select_fusion.1) | copy-start | bytes 393220
  261.3 9.5 %copy-start.1 = (f32[4,64,2,128]{3,1,0,2:T(8,128)S(1)}, f32[4,64,2,128]{3,1,0,2:T(8,128)}, u32[]{:S(2)}) copy-start(f32[4,64,2,128]{3,1,0,2:T(8,128)} %copy.263) | copy-start | bytes 786436
  261.3 9.6 %copy-start.11 = (f32[256,2,128]{2,0,1:T(8,128)S(1)}, f32[256,2,128]{2,0,1:T(8,128)}, u32[]{:S(2)}) copy-start(f32[256,2,128]{2,0,1:T(8,128)} %copy.280) | copy-start | bytes 786436
  261.3 9.7 %copy-start.12 = (f32[256,2,128]{2,0,1:T(8,128)S(1)}, f32[256,2,128]{2,0,1:T(8,128)}, u32[]{:S(2)}) copy-start(f32[256,2,128]{2,0,1:T(8,128)} %copy.320) | copy-start | bytes 786436
  261.3 9.7 %copy-start.25 = (f32[128]{0:T(128)S(1)}, f32[128]{0:T(128)}, u32[]{:S(2)}) copy-start(f32[128]{0:T(128)} %param.39) | copy-start | bytes 1540
  273.9 93.4 %all-gather.7.cloned.1.call-start = ((), (), s32[]{:S(2)}) async-start(), calls=%async_computation.3 | async-start | bytes 6488064 | tf_op jit(solution)/shard_map/all_gather | solution.py:245
  274.5 185.8 %all-gather.11.cloned.1.call-start = ((), (), s32[]{:S(2)}) async-start(), calls=%async_computation.5 | async-start | bytes 6488064 | tf_op jit(solution)/shard_map/all_gather | solution.py:251
  275.1 277.6 %all-gather.9.cloned.1.call-start = ((), (), s32[]{:S(2)}) async-start(), calls=%async_computation.4 | async-start | bytes 6488064 | tf_op jit(solution)/shard_map/all_gather | solution.py:246
  275.7 91.6 %copy-start.26 = (f32[2048]{0:T(1024)S(1)}, f32[2048]{0:T(1024)}, u32[]{:S(2)}) copy-start(f32[2048]{0:T(1024)} %param.42) | copy-start | bytes 24580
  275.7 310.0 %reduce-scatter.2.cloned.1.call-start = ((), (), s32[]{:S(2)}) async-start(), calls=%async_computation.6 | async-start | bytes 1310720 | tf_op jit(solution)/shard_map/reduce_scatter | solution.py:252
  (9 other events, 38.5 us)
Sparse Core Ops, SparseCore 0:
  274.0 35.1 all-reduce.1
  562.7 22.9 reduce-scatter.1
Sparse Core Ops, SparseCore 1:
  276.6 90.7 all-gather.6
  369.2 91.0 all-gather.10
  462.3 90.3 all-gather.8
